TPU v7x, 32 devices: a whole 2x2x4 slice. The times are simulated.
32 devices in a mesh: kv: 4 (over y, x), tp: 8 (over z, core).
Axes of the slice: x: 2, y: 2, z: 4, core: 2. Of those that a mesh axis runs over, the one named last changes fastest.
Arguments:
- tokens: bfloat16 [64, 4096], P('kv', 'tp'), may hold values from -6 to 6
- attn_gain: float32 [4096], replicated, may hold values from 0.1 to 1.9
- w_query: bfloat16 [4096, 2048], P(None, 'tp'), may hold values from -0.09375 to 0.09375
- w_key: bfloat16 [4096, 2048], P(None, 'tp'), may hold values from -0.09375 to 0.09375
- w_value: bfloat16 [4096, 2048], P(None, 'tp'), may hold values from -0.09375 to 0.09375
- w_outgate: bfloat16 [4096, 2048], P(None, 'tp'), may hold values from -0.09375 to 0.09375
- w_rates: bfloat16 [2, 4096, 16], P(None, None, 'tp'), may hold values from -0.09375 to 0.09375
- head_rate: float32 [16], P('tp'), may hold values from 0.02 to 2
- head_gain: float32 [2048], P('tp'), may hold values from 0.1 to 1.9
- w_out: bfloat16 [2048, 4096], P('tp'), may hold values from -0.125 to 0.125
- state: float32 [64, 16, 128, 128], P('kv', 'tp'), may hold values from -2.4 to 2.4
- mlp_gain: float32 [4096], replicated, may hold values from 0.1 to 1.9
- w_gate: bfloat16 [4096, 11264], P(None, ('kv', 'tp')), may hold values from -0.09375 to 0.09375
- w_up: bfloat16 [4096, 11264], P(None, ('kv', 'tp')), may hold values from -0.09375 to 0.09375
- w_down: bfloat16 [4096, 11264], P(None, ('kv', 'tp')), may hold values from -0.109375 to 0.109375
Outputs:
- result: bfloat16 [64, 4096], P('kv', 'tp')
- new_state: float32 [64, 16, 128, 128], P('kv', 'tp')
All inputs are finite; a program needn't handle non-finite values.
Results may differ from a plain program's by a relative error of at most 0.014.
Values may be sent and summed in bfloat16 or wider, within the bound.
A program may use at most 64 MiB of HBM per device.

v0:
```python
import jax
import jax.numpy as jnp
from jax import lax
from jax.sharding import PartitionSpec as P

EPS = 1e-06


def row_norm(values, gain):
    floats = values.astype(jnp.float32)
    scaled = floats * lax.rsqrt(jnp.mean(floats * floats, axis=-1, keepdims=True) + EPS)
    return (scaled * gain).astype(jnp.bfloat16)


def hidden_units(normed_mlp, gate_part, up_part):
    gate_pre = jnp.dot(normed_mlp, gate_part, preferred_element_type=jnp.float32)
    up_pre = jnp.dot(normed_mlp, up_part, preferred_element_type=jnp.float32)
    return (jax.nn.silu(gate_pre) * up_pre).astype(jnp.bfloat16)


def down_product(hidden, down_part):
    return lax.dot_general(
        hidden, down_part, (((1,), (1,)), ((), ())), preferred_element_type=jnp.float32
    )


def body(
    tokens,
    attn_gain,
    w_query,
    w_key,
    w_value,
    w_outgate,
    w_rates,
    head_rate,
    head_gain,
    w_out,
    state,
    mlp_gain,
    w_gate,
    w_up,
    w_down,
):
    count = tokens.shape[0]
    local_heads = head_rate.shape[0]
    size = w_query.shape[1] // local_heads
    whole_rows = lax.all_gather(tokens, "tp", axis=1, tiled=True)
    normed = row_norm(whole_rows, attn_gain)
    query = jnp.dot(normed, w_query, preferred_element_type=jnp.float32).reshape(
        count, local_heads, size
    )
    key = jnp.dot(normed, w_key, preferred_element_type=jnp.float32).reshape(
        count, local_heads, size
    )
    value = jnp.dot(normed, w_value, preferred_element_type=jnp.float32).reshape(
        count, local_heads, size
    )
    gate_in = jnp.dot(normed, w_outgate, preferred_element_type=jnp.float32).reshape(
        count, local_heads, size
    )
    rates = jnp.einsum("bd,sdh->sbh", normed, w_rates, preferred_element_type=jnp.float32)
    unit_query = (
        query * lax.rsqrt(jnp.sum(query * query, axis=-1, keepdims=True) + EPS) * size ** (-0.5)
    )
    unit_key = key * lax.rsqrt(jnp.sum(key * key, axis=-1, keepdims=True) + EPS)
    strength = jax.nn.sigmoid(rates[0])
    fade = jnp.exp(-head_rate * jax.nn.softplus(rates[1]))
    carried = state * fade[:, :, None, None]
    fresh = strength[:, :, None] * (value - jnp.einsum("bhi,bhiv->bhv", unit_key, carried))
    new_state = carried + unit_key[:, :, :, None] * fresh[:, :, None, :]
    readout = jnp.einsum("bhi,bhiv->bhv", unit_query, new_state)
    normed_out = readout * lax.rsqrt(jnp.mean(readout * readout, axis=-1, keepdims=True) + EPS)
    mixed = (normed_out * head_gain.reshape(local_heads, size) * jax.nn.silu(gate_in)).astype(
        jnp.bfloat16
    )
    partial_value = jnp.dot(
        mixed.reshape(count, local_heads * size), w_out, preferred_element_type=jnp.float32
    )
    projected = lax.psum_scatter(partial_value, "tp", scatter_dimension=1, tiled=True)
    residual = (tokens.astype(jnp.float32) + projected).astype(jnp.bfloat16)
    full_residual = lax.all_gather(residual, "tp", axis=1, tiled=True)
    normed_mlp = row_norm(full_residual, mlp_gain)
    shared_rows = lax.all_gather(normed_mlp, "kv", axis=0, tiled=True)
    hidden = hidden_units(shared_rows, w_gate, w_up)
    owned = lax.all_to_all(hidden, "kv", split_axis=0, concat_axis=1, tiled=True)
    folded = down_product(owned, lax.all_gather(w_down, "kv", axis=1, tiled=True))
    down = lax.psum_scatter(folded, "tp", scatter_dimension=1, tiled=True)
    result = (residual.astype(jnp.float32) + down).astype(jnp.bfloat16)
    return (result, new_state)


def solution(mesh):
    return jax.shard_map(
        body,
        mesh=mesh,
        in_specs=(
            P("kv", "tp"),
            P(),
            P(None, "tp"),
            P(None, "tp"),
            P(None, "tp"),
            P(None, "tp"),
            P(None, None, "tp"),
            P("tp"),
            P("tp"),
            P("tp", None),
            P("kv", "tp", None, None),
            P(),
            P(None, ("kv", "tp")),
            P(None, ("kv", "tp")),
            P(None, ("kv", "tp")),
        ),
        out_specs=(P("kv", "tp"), P("kv", "tp", None, None)),
        check_vma=False,
    )
```

profile of v0, /device:TPU:0, one launch (start us, length us, event | category | flops | bytes accessed | tf_op | source)
XLA Modules:
  0.0 203.6 jit_solution(17371665273505232595)
XLA Ops:
  8.1 16.1 %all_gather.12 = bf16[16,4096]{1,0:T(8,128)(2,1)S(1)} all-gather(bf16[16,512]{1,0:T(8,128)(2,1)} %param.15), channel_id=1, replica_groups=mesh['kv'=4,'tp'=8] {'tp'}, dimensions={1}, use_global_device_ids=true | all-gather | bytes 147456 | tf_op jit(solution)/shard_map/all_gather | solution.py:47
  24.2 0.1 fusion.4
  24.3 2.0 fusion.26
  26.4 0.1 multiply_reduce_fusion.1
  26.6 0.2 convolution_bitcast_fusion
  27.1 2.0 fusion.24
  29.2 2.2 %fusion = f32[16,2,1,128]{3,2,1,0:T(1,128)S(1)} fusion(f32[16,2,128,1]{2,3,1,0:T(1,128)S(1)} %bitcast.46, f32[16,2,128,128]{3,2,1,0:T(8,128)} %param.25, f32[16,2]{1,0:T(8,128)S(1)} %copy.22), kind=kOutput, calls=%fused_computation.1 | convolution fusion | flops 1572864 | bytes 2130048 | tf_op jit(solution)/shard_map/bhi,bhiv->bhv/dot_general | solution.py:69
  31.3 0.1 subtract_multiply_fusion
  31.5 1.7 multiply_add_fusion
  33.2 0.4 copy-done.3
  33.6 0.4 fusion.29
  34.1 0.1 multiply_reduce_fusion.2
  34.3 2.1 %fusion.31 = f32[16,2,1,128]{3,2,1,0:T(1,128)S(1)} fusion(f32[16,2,128,1]{2,3,1,0:T(1,128)S(1)} %bitcast.50, f32[16,2,128,128]{3,2,1,0:T(8,128)} %multiply_add_fusion), kind=kOutput, calls=%fused_computation.50 | convolution fusion | flops 1048576 | bytes 2129920 | tf_op jit(solution)/shard_map/bhi,bhiv->bhv/dot_general | solution.py:71
  36.4 0.1 multiply_reduce_fusion
  36.5 0.4 fusion.22
  36.9 0.1 fusion.12
  37.0 2.7 %fusion.13 = f32[16,4096]{1,0:T(8,128)} fusion(bf16[256,4096]{1,0:T(8,128)(2,1)} %param.24, bf16[2,8,2,128]{3,2,1,0:T(2,128)(2,1)S(1)} %bitcast.51), kind=kOutput, calls=%fused_computation.28 | convolution fusion | flops 33554432 | bytes 2367488 | tf_op jit(solution)/shard_map/dot_general | solution.py:76
  39.8 0.5 all-gather.2.cloned.1.call-update
  40.4 31.3 %reduce-scatter.3.cloned.1.call-done = f32[16,512]{1,0:T(8,128)} async-done(((f32[16,4096]{1,0:T(8,128)}), f32[16,512]{1,0:T(8,128)}) %reduce-scatter.3.cloned.1.call-update) | async-done | bytes 32784 | tf_op jit(solution)/shard_map/reduce_scatter | solution.py:79
  71.7 0.8 add_convert_fusion.1
  72.5 13.9 %all_gather.13 = bf16[16,4096]{1,0:T(8,128)(2,1)S(1)} all-gather(bf16[16,512]{1,0:T(8,128)(2,1)S(1)} %add_convert_fusion.1), channel_id=1, replica_groups=mesh['kv'=4,'tp'=8] {'tp'}, dimensions={1}, use_global_device_ids=true | all-gather | bytes 147456 | tf_op jit(solution)/shard_map/all_gather | solution.py:81
  86.4 0.1 fusion.7
  86.6 0.1 fusion.9
  86.7 13.8 %all_gather.14 = bf16[64,4096]{1,0:T(8,128)(2,1)S(1)} all-gather(bf16[16,4096]{1,0:T(8,128)(2,1)S(1)} %fusion.9), channel_id=1, replica_groups=mesh['kv'=4,'tp'=8] {'kv'}, dimensions={0}, use_global_device_ids=true | all-gather | bytes 655360 | tf_op jit(solution)/shard_map/all_gather | solution.py:83
  100.5 0.9 fusion.32
  101.5 0.9 fusion.2
  102.4 8.0 %all_to_all.19 = bf16[4,16,352]{2,1,0:T(8,128)(2,1)S(1)} all-to-all(bf16[4,16,352]{2,1,0:T(8,128)(2,1)S(1)} %bitcast.44), channel_id=1, replica_groups=mesh['kv'=4,'tp'=8] {'kv'}, dimensions={0} | all-to-all | bytes 90112 | tf_op jit(solution)/shard_map/all_to_all | solution.py:85
  110.5 0.1 all_to_all.17
  110.6 49.2 %all-gather.2.cloned.1.call-done = bf16[4096,1408]{0,1:T(8,128)(2,1)} async-done(((bf16[4096,352]{0,1:T(8,128)(2,1)}), bf16[4096,1408]{0,1:T(8,128)(2,1)}) %all-gather.2.cloned.1.call-update) | async-done | bytes 11534352 | tf_op jit(solution)/shard_map/all_gather | solution.py:86
  159.8 6.6 %fusion.33 = f32[16,4096]{1,0:T(8,128)} fusion(bf16[16,1408]{1,0:T(8,128)(2,1)S(1)} %all_to_all.17, bf16[4096,1408]{0,1:T(8,128)(2,1)} %all-gather.2.cloned.1.call-done), kind=kOutput, calls=%fused_computation.52 | convolution fusion | flops 184549376 | bytes 11841536 | tf_op jit(solution)/shard_map/dot_general | solution.py:22
  166.4 28.4 %reduce-scatter.5.cloned.1.call-done = f32[16,512]{1,0:T(8,128)} async-done(((f32[16,4096]{1,0:T(8,128)}), f32[16,512]{1,0:T(8,128)}) %reduce-scatter.5.cloned.1.call-update) | async-done | bytes 32784 | tf_op jit(solution)/shard_map/reduce_scatter | solution.py:87
  194.8 1.4 add_convert_fusion
  (43 shorter events, 0.8 us)
Async XLA Ops:
  8.0 92.5 %copy-start = (bf16[4096,352]{0,1:T(8,128)(2,1)S(1)}, bf16[4096,352]{0,1:T(8,128)(2,1)}, u32[]{:S(2)}) copy-start(bf16[4096,352]{0,1:T(8,128)(2,1)} %param.27) | copy-start | bytes 8650756
  8.0 18.6 %copy-start.5 = (f32[4096]{0:T(1024)S(1)}, f32[4096]{0:T(1024)}, u32[]{:S(2)}) copy-start(f32[4096]{0:T(1024)} %param.16) | copy-start | bytes 49156
  8.0 18.6 %copy-start.9 = (bf16[2,4096,2]{1,2,0:T(2,128)(2,1)S(1)}, bf16[2,4096,2]{1,2,0:T(2,128)(2,1)}, u32[]{:S(2)}) copy-start(bf16[2,4096,2]{1,2,0:T(2,128)(2,1)} %param.21) | copy-start | bytes 98308
  8.0 18.8 %copy-start.10 = (f32[2]{0:T(128)S(1)}, f32[2]{0:T(128)}, u32[]{:S(2)}) copy-start(f32[2]{0:T(128)} %param.22) | copy-start | bytes 28
  8.0 63.6 %reduce-scatter.3.cloned.1.call-start = ((), (), s32[]{:S(2)}) async-start(), calls=%async_computation.3 | async-start | bytes 294912 | tf_op jit(solution)/shard_map/reduce_scatter | solution.py:79
  29.2 2.3 %copy-start.1 = (f32[16,2,128,128]{3,2,1,0:T(8,128)S(1)}, f32[16,2,128,128]{3,2,1,0:T(8,128)}, u32[]{:S(2)}) copy-start(f32[16,2,128,128]{3,2,1,0:T(8,128)} %param.25) | copy-start | bytes 6291460
  31.5 2.2 %copy-start.3 = (bf16[4096,256]{1,0:T(8,128)(2,1)S(1)}, bf16[4096,256]{1,0:T(8,128)(2,1)}, u32[]{:S(2)}) copy-start(bf16[4096,256]{1,0:T(8,128)(2,1)} %param.17) | copy-start | bytes 6291460
  34.1 2.4 %copy-start.4 = (bf16[4096,256]{1,0:T(8,128)(2,1)S(1)}, bf16[4096,256]{1,0:T(8,128)(2,1)}, u32[]{:S(2)}) copy-start(bf16[4096,256]{1,0:T(8,128)(2,1)} %param.20) | copy-start | bytes 6291460
  34.3 2.7 %copy-start.8 = (f32[256]{0:T(256)S(1)}, f32[256]{0:T(256)}, u32[]{:S(2)}) copy-start(f32[256]{0:T(256)} %param.23) | copy-start | bytes 3076
  39.7 32.0 %copy-start.6 = (bf16[16,512]{1,0:T(8,128)(2,1)S(1)}, bf16[16,512]{1,0:T(8,128)(2,1)}, u32[]{:S(2)}) copy-start(bf16[16,512]{1,0:T(8,128)(2,1)} %param.15) | copy-start | bytes 49156
  39.7 46.8 %copy-start.7 = (f32[4096]{0:T(1024)S(1)}, f32[4096]{0:T(1024)}, u32[]{:S(2)}) copy-start(f32[4096]{0:T(1024)} %param.26) | copy-start | bytes 49156
  39.8 120.0 %all-gather.2.cloned.1.call-start = ((), (), s32[]{:S(2)}) async-start(), calls=%async_computation.4 | async-start | bytes 14417920 | tf_op jit(solution)/shard_map/all_gather | solution.py:86
  40.3 154.4 %reduce-scatter.5.cloned.1.call-start = ((), (), s32[]{:S(2)}) async-start(), calls=%async_computation.5 | async-start | bytes 294912 | tf_op jit(solution)/shard_map/reduce_scatter | solution.py:87
  86.7 14.8 %copy-start.2 = (bf16[4096,352]{0,1:T(8,128)(2,1)S(1)}, bf16[4096,352]{0,1:T(8,128)(2,1)}, u32[]{:S(2)}) copy-start(bf16[4096,352]{0,1:T(8,128)(2,1)} %param.28) | copy-start | bytes 8650756
Sparse Core Ops, SparseCore 0:
  39.9 31.7 reduce-scatter.2
  166.5 28.2 reduce-scatter.4
Sparse Core Ops, SparseCore 1:
  42.1 117.6 all-gather.1
where the time goes:
time: 204 us
  waiting for transfers between devices  109 us (53%)
  blocking collectives  51.9 us (25%)
  matrix products  20.5 us (10%)
  between operations  15.7 us (8%)
  other arithmetic  4.97 us (2%)
    all_gather x1, waiting for transfers between devices, body(): lax.all_gather(w_down, 'kv', axis=1, tiled=True)  49.2 us
    reduce_scatter x1, waiting for transfers between devices, body(): lax.psum_scatter(partial_value, 'tp', scatter_dimension=1, tiled=True)  31.3 us
    reduce_scatter x1, waiting for transfers between devices, body(): down = lax.psum_scatter(folded, 'tp', scatter_dimension=1, tiled=True)  28.4 us
    all_gather x1, blocking collectives, body(): whole_rows = lax.all_gather(tokens, 'tp', axis=1, tiled=True)  16.1 us
    all_gather x1, blocking collectives, body(): full_residual = lax.all_gather(residual, 'tp', axis=1, tiled=True)  13.9 us
    all_gather x1, blocking collectives, body(): shared_rows = lax.all_gather(normed_mlp, 'kv', axis=0, tiled=True)  13.8 us
    all_to_all x1, blocking collectives, body(): lax.all_to_all(hidden, 'kv', split_axis=0, concat_axis=1, tiled=True)  8.03 us
    dot_general x1, matrix products, down_product(): lax.dot_general(hidden, down_part, (((1,), (1,)), ((), ())), preferred_el...  6.59 us
  transfers between devices with their start and end apart: 3, of which 3 were waited for; matrix products, arithmetic and copies ran while one was open for 1% of the time, Pallas kernels for 0%

commit v1 on v0

v1 whole, which is shorter than its diff:
```python
import functools

import jax
import jax.numpy as jnp
from jax import lax
from jax.experimental import pallas as pl
from jax.experimental.pallas import tpu as pltpu
from jax.sharding import PartitionSpec as P

EPS = 1e-06
MESH = pl.DeviceIdType.MESH
NT = (((1,), (1,)), ((), ()))


def remote(src, dst, send_sem, recv_sem, kv, tp):
    return pltpu.make_async_remote_copy(
        src_ref=src,
        dst_ref=dst,
        send_sem=send_sem,
        recv_sem=recv_sem,
        device_id=(kv, tp),
        device_id_type=MESH,
    )


def layer_kernel(
    kv_count,
    tp_count,
    tokens_hbm,
    attn_gain_hbm,
    w_query_hbm,
    w_key_hbm,
    w_value_hbm,
    w_outgate_hbm,
    w_rates_hbm,
    head_rate_ref,
    head_gain_ref,
    w_out_hbm,
    state_hbm,
    mlp_gain_hbm,
    w_gate_hbm,
    w_up_hbm,
    w_down_hbm,
    result_ref,
    new_state_hbm,
    attn_gain,
    w_query,
    w_key,
    w_value,
    w_outgate,
    w_rates,
    w_out,
    state,
    mlp_gain,
    w_gate,
    w_up,
    w_down,
    rows_all,
    share_out,
    share_in,
    res_all,
    pair_out,
    pair_in,
    total,
    group_out,
    group_in,
    last_out,
    last_in,
    load_sem,
    store_sem,
    rows_send,
    rows_recv,
    share_send,
    share_recv,
    res_send_z,
    res_send_kv,
    res_send_pair,
    res_recv,
    pair_send,
    pair_recv,
    group_send,
    group_recv,
    last_send,
    last_recv,
):
    kv = lax.axis_index("kv")
    tp = lax.axis_index("tp")
    z_count = tp_count // 2
    z = tp // 2
    core = tp % 2
    partner = tp + 1 - 2 * core
    count, width = tokens_hbm.shape
    heads = state_hbm.shape[1]
    size = state_hbm.shape[2]
    model = width * tp_count

    def z_peer(step):
        return lax.rem(z + step, z_count)

    def kv_peer(step):
        return lax.rem(kv + step, kv_count)

    own_rows = pltpu.make_async_copy(tokens_hbm, rows_all.at[tp], load_sem.at[0])
    own_rows.start()
    pairs = [
        (attn_gain_hbm, attn_gain),
        (w_rates_hbm, w_rates),
        (w_query_hbm, w_query),
        (w_key_hbm, w_key),
        (w_value_hbm, w_value),
        (w_outgate_hbm, w_outgate),
        (state_hbm, state),
        (w_out_hbm, w_out),
        (mlp_gain_hbm, mlp_gain),
        (w_gate_hbm, w_gate),
        (w_up_hbm, w_up),
        (w_down_hbm, w_down),
    ]
    loads = []
    for index, (source, target) in enumerate(pairs):
        load = pltpu.make_async_copy(source, target, load_sem.at[index + 1])
        load.start()
        loads.append(load)

    barrier = pltpu.get_barrier_semaphore()
    for step in range(1, tp_count):
        pl.semaphore_signal(
            barrier, inc=1, device_id=(kv, lax.rem(tp + step, tp_count)), device_id_type=MESH
        )
    for step in range(1, kv_count):
        pl.semaphore_signal(barrier, inc=1, device_id=(kv_peer(step), tp), device_id_type=MESH)
    pl.semaphore_wait(barrier, tp_count - 1 + kv_count - 1)

    own_rows.wait()
    sent = []
    for step in range(1, tp_count):
        copy = remote(
            rows_all.at[tp],
            rows_all.at[tp],
            rows_send.at[step],
            rows_recv.at[tp],
            kv,
            lax.rem(tp + step, tp_count),
        )
        copy.start()
        sent.append(copy)
    for step in range(1, tp_count):
        source = lax.rem(tp + step, tp_count)
        remote(
            rows_all.at[source],
            rows_all.at[source],
            rows_send.at[step],
            rows_recv.at[source],
            kv,
            source,
        ).wait_recv()

    loads[0].wait()
    loads[1].wait()
    squares = jnp.zeros((count, width), jnp.float32)
    write_sums = [jnp.zeros((count, width), jnp.float32) for _ in range(heads)]
    decay_sums = [jnp.zeros((count, width), jnp.float32) for _ in range(heads)]
    scaled = []
    for block in range(tp_count):
        columns = slice(block * width, (block + 1) * width)
        floats = rows_all[block].astype(jnp.float32)
        squares += floats * floats
        floats = floats * attn_gain[:, columns]
        for head in range(heads):
            write_sums[head] += floats * w_rates[0, head : head + 1, columns].astype(jnp.float32)
            decay_sums[head] += floats * w_rates[1, head : head + 1, columns].astype(jnp.float32)
        scaled.append(floats.astype(jnp.bfloat16))
    norm = lax.rsqrt(jnp.sum(squares, axis=-1, keepdims=True) / model + EPS)

    def project(weight):
        product = jnp.zeros((count, heads * size), jnp.float32)
        for block in range(tp_count):
            product += jnp.dot(
                scaled[block],
                weight[block * width : (block + 1) * width, :],
                preferred_element_type=jnp.float32,
            )
        return product * norm

    loads[2].wait()
    query = project(w_query)
    loads[3].wait()
    key = project(w_key)
    loads[4].wait()
    value = project(w_value)
    loads[5].wait()
    gate_in = project(w_outgate)

    loads[6].wait()
    mixed = []
    for head in range(heads):
        lanes = slice(head * size, (head + 1) * size)
        query_h = query[:, lanes]
        key_h = key[:, lanes]
        unit_query = (
            query_h
            * lax.rsqrt(jnp.sum(query_h * query_h, axis=-1, keepdims=True) + EPS)
            * size ** (-0.5)
        )
        unit_key = key_h * lax.rsqrt(jnp.sum(key_h * key_h, axis=-1, keepdims=True) + EPS)
        write_raw = jnp.sum(write_sums[head], axis=-1, keepdims=True) * norm
        decay_raw = jnp.sum(decay_sums[head], axis=-1, keepdims=True) * norm
        strength = jnp.broadcast_to(jax.nn.sigmoid(write_raw), (count, size))
        rate = head_rate_ref[:, head : head + 1]
        softplus = jnp.maximum(decay_raw, 0.0) + jnp.log1p(jnp.exp(-jnp.abs(decay_raw)))
        fade = jnp.broadcast_to(jnp.exp(-rate * softplus), (count, size))
        query_t = unit_query.T
        key_t = unit_key.T
        rows = []
        for row in range(count):
            here = slice(row, row + 1)
            key_column = key_t[:, here]
            carried = state[row, head] * fade[here, :]
            recalled = jnp.sum(carried * key_column, axis=0, keepdims=True)
            fresh = strength[here, :] * (value[here, lanes] - recalled)
            updated = carried + key_column * fresh
            state[row, head] = updated
            rows.append(jnp.sum(updated * query_t[:, here], axis=0, keepdims=True))
        readout = jnp.concatenate(rows, axis=0)
        normed_out = readout * lax.rsqrt(
            jnp.mean(readout * readout, axis=-1, keepdims=True) + EPS
        )
        gate_h = gate_in[:, lanes]
        silu = gate_h / (1.0 + jnp.exp(-gate_h))
        mixed.append((normed_out * head_gain_ref[:, lanes] * silu).astype(jnp.bfloat16))
    store = pltpu.make_async_copy(state, new_state_hbm, store_sem)
    store.start()

    loads[7].wait()

    def out_block(owner):
        columns = pl.ds(pl.multiple_of(owner * width, width), width)
        product = jnp.zeros((count, width), jnp.float32)
        for head in range(heads):
            product += jnp.dot(
                mixed[head],
                w_out[head * size : (head + 1) * size, columns],
                preferred_element_type=jnp.float32,
            )
        return product

    for step in range(1, tp_count):
        owner = lax.rem(tp + step, tp_count)
        share_out[step] = out_block(owner).astype(jnp.bfloat16)
        copy = remote(
            share_out.at[step],
            share_in.at[tp],
            share_send.at[step],
            share_recv.at[tp],
            kv,
            owner,
        )
        copy.start()
        sent.append(copy)
    residual = rows_all[tp].astype(jnp.float32) + out_block(tp)
    for step in range(1, tp_count):
        source = lax.rem(tp + step, tp_count)
        remote(
            share_out.at[step],
            share_in.at[source],
            share_send.at[step],
            share_recv.at[source],
            kv,
            source,
        ).wait_recv()
        residual += share_in[source].astype(jnp.float32)
    residual = residual.astype(jnp.bfloat16)
    res_all[tp, kv] = residual

    def pass_on(block, group, send_sem, to_kv, to_tp):
        copy = remote(
            res_all.at[block, group],
            res_all.at[block, group],
            send_sem,
            res_recv.at[block, group],
            to_kv,
            to_tp,
        )
        copy.start()
        sent.append(copy)

    def arrival(block, group):
        remote(
            res_all.at[block, group],
            res_all.at[block, group],
            res_send_z.at[0],
            res_recv.at[block, group],
            kv,
            partner,
        ).wait_recv()

    for step in range(1, z_count):
        pass_on(tp, kv, res_send_z.at[step], kv, 2 * z_peer(step) + core)
    for step in range(1, kv_count):
        pass_on(tp, kv, res_send_kv.at[0, step], kv_peer(step), tp)
    pass_on(tp, kv, res_send_pair.at[0, 0], kv, partner)
    for z_step in range(1, z_count):
        block = 2 * z_peer(z_step) + core
        arrival(block, kv)
        for step in range(1, kv_count):
            pass_on(block, kv, res_send_kv.at[z_step, step], kv_peer(step), tp)
        pass_on(block, kv, res_send_pair.at[z_step, 0], kv, partner)
    for z_step in range(z_count):
        block = 2 * z_peer(z_step) + core
        for step in range(1, kv_count):
            arrival(block, kv_peer(step))
            pass_on(block, kv_peer(step), res_send_pair.at[z_step, step], kv, partner)
    for z_step in range(z_count):
        block = 2 * z_peer(z_step) + 1 - core
        for step in range(kv_count):
            arrival(block, kv_peer(step))

    everyone = kv_count * count
    units = w_gate_hbm.shape[0]
    for index in (8, 9, 10):
        loads[index].wait()
    squares = jnp.zeros((everyone, width), jnp.float32)
    gate_pre = jnp.zeros((everyone, units), jnp.float32)
    up_pre = jnp.zeros((everyone, units), jnp.float32)
    for block in range(tp_count):
        columns = slice(block * width, (block + 1) * width)
        floats = res_all[block].reshape(everyone, width).astype(jnp.float32)
        squares += floats * floats
        part = (floats * mlp_gain[:, columns]).astype(jnp.bfloat16)
        gate_pre += lax.dot_general(
            part, w_gate[:, columns], NT, preferred_element_type=jnp.float32
        )
        up_pre += lax.dot_general(part, w_up[:, columns], NT, preferred_element_type=jnp.float32)
    norm = lax.rsqrt(jnp.sum(squares, axis=-1, keepdims=True) / model + EPS)
    gate_pre = gate_pre * norm
    hidden = (gate_pre / (1.0 + jnp.exp(-gate_pre)) * (up_pre * norm)).astype(jnp.bfloat16)
    loads[11].wait()

    def down_block(owner):
        columns = pl.ds(pl.multiple_of(owner * width, width), width)
        product = jnp.dot(hidden, w_down[:, columns], preferred_element_type=jnp.float32)
        return product.reshape(kv_count, count, width)

    for step in range(z_count):
        there = z_peer(step)
        pair_out[step] = down_block(2 * there + 1 - core).astype(jnp.bfloat16)
        copy = remote(
            pair_out.at[step],
            pair_in.at[there],
            pair_send.at[step],
            pair_recv.at[there],
            kv,
            partner,
        )
        copy.start()
        sent.append(copy)
    for step in range(z_count):
        there = z_peer(step)
        total[there] = down_block(2 * there + core)
    order = [step for step in range(1, z_count)] + [0]
    for step in order:
        there = z_peer(step)
        remote(
            pair_out.at[step],
            pair_in.at[there],
            pair_send.at[step],
            pair_recv.at[there],
            kv,
            partner,
        ).wait_recv()
        for kv_step in range(1, kv_count):
            group = kv_peer(kv_step)
            both = total[there, group] + pair_in[there, group].astype(jnp.float32)
            group_out[there, group] = both.astype(jnp.bfloat16)
            copy = remote(
                group_out.at[there, group],
                group_in.at[there, kv],
                group_send.at[step, kv_step],
                group_recv.at[there, kv],
                group,
                tp,
            )
            copy.start()
            sent.append(copy)
    mine = None
    for step in order:
        there = z_peer(step)
        both = total[there, kv] + pair_in[there, kv].astype(jnp.float32)
        for kv_step in range(1, kv_count):
            group = kv_peer(kv_step)
            remote(
                group_out.at[there, group],
                group_in.at[there, group],
                group_send.at[step, kv_step],
                group_recv.at[there, group],
                group,
                tp,
            ).wait_recv()
            both += group_in[there, group].astype(jnp.float32)
        if step == 0:
            mine = both
            continue
        last_out[step] = both.astype(jnp.bfloat16)
        copy = remote(
            last_out.at[step],
            last_in.at[z],
            last_send.at[step],
            last_recv.at[z],
            kv,
            2 * there + core,
        )
        copy.start()
        sent.append(copy)
    mine += residual.astype(jnp.float32)
    for step in range(1, z_count):
        there = z_peer(step)
        remote(
            last_out.at[step],
            last_in.at[there],
            last_send.at[step],
            last_recv.at[there],
            kv,
            2 * there + core,
        ).wait_recv()
        mine += last_in[there].astype(jnp.float32)
    result_ref[...] = mine.astype(jnp.bfloat16)

    for copy in sent:
        copy.wait_send()
    store.wait()


def body(
    kv_count,
    tp_count,
    tokens,
    attn_gain,
    w_query,
    w_key,
    w_value,
    w_outgate,
    w_rates,
    head_rate,
    head_gain,
    w_out,
    state,
    mlp_gain,
    w_gate,
    w_up,
    w_down,
):
    count, width = tokens.shape
    heads = head_rate.shape[0]
    z_count = tp_count // 2
    operands = (
        tokens,
        attn_gain.reshape(1, -1),
        w_query,
        w_key,
        w_value,
        w_outgate,
        w_rates.transpose(0, 2, 1),
        head_rate.reshape(1, -1),
        head_gain.reshape(1, -1),
        w_out,
        state,
        mlp_gain.reshape(1, -1),
        w_gate.T,
        w_up.T,
        w_down.T,
    )
    in_vmem = (7, 8)
    anywhere = pl.BlockSpec(memory_space=pl.ANY)
    vmem = pl.BlockSpec(memory_space=pltpu.VMEM)
    local = [
        pltpu.VMEM(operands[index].shape, operands[index].dtype)
        for index in (1, 2, 3, 4, 5, 6, 9, 10, 11, 12, 13, 14)
    ]
    bf16 = jnp.bfloat16
    dma = pltpu.SemaphoreType.DMA
    exchange = [
        pltpu.VMEM((tp_count, count, width), bf16),
        pltpu.VMEM((tp_count, count, width), bf16),
        pltpu.VMEM((tp_count, count, width), bf16),
        pltpu.VMEM((tp_count, kv_count, count, width), bf16),
        pltpu.VMEM((z_count, kv_count, count, width), bf16),
        pltpu.VMEM((z_count, kv_count, count, width), bf16),
        pltpu.VMEM((z_count, kv_count, count, width), jnp.float32),
        pltpu.VMEM((z_count, kv_count, count, width), bf16),
        pltpu.VMEM((z_count, kv_count, count, width), bf16),
        pltpu.VMEM((z_count, count, width), bf16),
        pltpu.VMEM((z_count, count, width), bf16),
        dma((len(local) + 1,)),
        dma,
        dma((tp_count,)),
        dma((tp_count,)),
        dma((tp_count,)),
        dma((tp_count,)),
        dma((z_count,)),
        dma((z_count, kv_count)),
        dma((z_count, kv_count)),
        dma((tp_count, kv_count)),
        dma((z_count,)),
        dma((z_count,)),
        dma((z_count, kv_count)),
        dma((z_count, kv_count)),
        dma((z_count,)),
        dma((z_count,)),
    ]
    return pl.pallas_call(
        functools.partial(layer_kernel, kv_count, tp_count),
        out_shape=(
            jax.ShapeDtypeStruct(tokens.shape, bf16),
            jax.ShapeDtypeStruct(state.shape, jnp.float32),
        ),
        in_specs=[vmem if index in in_vmem else anywhere for index in range(len(operands))],
        out_specs=(vmem, anywhere),
        scratch_shapes=local + exchange,
        compiler_params=pltpu.CompilerParams(
            collective_id=0, has_side_effects=True, vmem_limit_bytes=60 * 1024 * 1024
        ),
        name="layer",
    )(*operands)


def solution(mesh):
    return jax.shard_map(
        functools.partial(body, mesh.shape["kv"], mesh.shape["tp"]),
        mesh=mesh,
        in_specs=(
            P("kv", "tp"),
            P(),
            P(None, "tp"),
            P(None, "tp"),
            P(None, "tp"),
            P(None, "tp"),
            P(None, None, "tp"),
            P("tp"),
            P("tp"),
            P("tp", None),
            P("kv", "tp", None, None),
            P(),
            P(None, ("kv", "tp")),
            P(None, ("kv", "tp")),
            P(None, ("kv", "tp")),
        ),
        out_specs=(P("kv", "tp"), P("kv", "tp", None, None)),
        check_vma=False,
    )
```

time: 204 us -> 47.4 us (0.23)
  waiting for transfers between devices: 109 us -> 0 us
  blocking collectives: 51.9 us -> 0 us
  Pallas kernels: 0 us -> 42 us
  matrix products: 20.5 us -> 0 us
  between operations: 15.7 us -> 0.64 us
  other arithmetic: 4.97 us -> 0 us
  local copies, waits for them, and re-layouts: 0.86 us -> 4.46 us
    reduce_scatter x2 -> x0, waiting for transfers between devices: 59.7 us -> none  [the longest x1 31.3 us: body(): lax.psum_scatter(partial_value, 'tp', scatter_dimension=1, tiled=True)]
    all_gather x1 -> x0, waiting for transfers between devices: 49.2 us -> none  [body(): lax.all_gather(w_down, 'kv', axis=1, tiled=True)]
    all_gather x3 -> x0, blocking collectives: 43.8 us -> none  [the longest x1 16.1 us: body(): whole_rows = lax.all_gather(tokens, 'tp', axis=1, tiled=True)]
    pallas_call x0 -> x1, Pallas kernels: none -> 42 us  [body(): pl.pallas_call(functools.partial(layer_kernel, kv_count, tp_count), out_s...]
    dot_general x11 -> x0, matrix products: 20.5 us -> none  [the longest x1 6.59 us: down_product(): lax.dot_general(hidden, down_part, (((1,), (1,)), ((), ())), preferred_el...]
    all_to_all x1 -> x0, blocking collectives: 8.03 us -> none  [body(): lax.all_to_all(hidden, 'kv', split_axis=0, concat_axis=1, tiled=True)]
    unnamed x22 -> x2, local copies, waits for them, and re-layouts: 0.5 us -> 4.46 us
    convert_element_type x4 -> x0, other arithmetic: 2.32 us -> none  [the longest x1 1.37 us: body(): result = (residual.astype(jnp.float32) + down).astype(jnp.bfloat16)]
  transfers between devices with their start and end apart: 3 -> 0, of which waited for: 3 -> 0; matrix products, arithmetic and copies ran while one was open for 1% -> 0% of each run, Pallas kernels for 0% -> 0%
where the time goes in v1:
time: 47.4 us; the launch traced here: 47.1 us
  Pallas kernels  42 us (89%)
  local copies, waits for them, and re-layouts  4.46 us (9%)
  between operations  0.64 us (1%)
    pallas_call x1, Pallas kernels, body(): pl.pallas_call(functools.partial(layer_kernel, kv_count, tp_count), out_s...  42 us
    unnamed x2, local copies, waits for them, and re-layouts  4.46 us

profile of v1, /device:TPU:0, one launch (start us, length us, event | category | flops | bytes accessed | tf_op | source)
XLA Modules:
  0.0 47.1 jit_solution(3491182717204539240)
XLA Ops:
  0.6 42.0 %layer.1 = (bf16[16,512]{1,0:T(8,128)(2,1)}, f32[16,2,128,128]{3,2,1,0:T(8,128)}) custom-call(bf16[16,512]{1,0:T(8,128)(2,1)} %tokens_hbm.1, f32[1,4096]{1,0:T(1,128)} %bitcast.12, bf16[4096,256]{1,0:T(8,128)(2,1)} %w_query_hbm.1, bf16[4096,256]{1,0:T(8,128)(2,1)} %w_key_hbm.1, bf16[4096,256]{1,0:T(8,128)(2,1)} %w_value_hbm.1, ...), custom_call_target="tpu_custom_call" | custom-call | tf_op jit(solution)/shard_map/layer/pallas_call | solution.py:510
  42.6 1.3 %copy.19 = bf16[16,512]{1,0:T(8,128)(2,1)} copy(bf16[16,512]{1,0:T(8,128)(2,1)} %get-tuple-element.4) | data formatting | bytes 32768
  44.0 3.1 %copy.20 = f32[16,2,128,128]{3,2,1,0:T(8,128)} copy(f32[16,2,128,128]{3,2,1,0:T(8,128)} %get-tuple-element.5) | data formatting | bytes 4194304

commit v2 on v1

--- a/solution.py
+++ b/solution.py
@@ -21,6 +21,17 @@
         device_id=(kv, tp),
         device_id_type=MESH,
     )
+
+
+def paired(index, step, count):
+    if count & (count - 1):
+        return lax.rem(index + step, count)
+    bit = 1
+    while bit < count:
+        if step & bit:
+            index = index + bit - 2 * bit * ((index // bit) % 2)
+        bit *= 2
+    return index
 
 
 def layer_kernel(
@@ -42,7 +53,7 @@
     w_up_hbm,
     w_down_hbm,
     result_ref,
-    new_state_hbm,
+    new_state,
     attn_gain,
     w_query,
     w_key,
@@ -67,7 +78,6 @@
     last_out,
     last_in,
     load_sem,
-    store_sem,
     rows_send,
     rows_recv,
     share_send,
@@ -95,10 +105,13 @@
     model = width * tp_count
 
     def z_peer(step):
-        return lax.rem(z + step, z_count)
+        return paired(z, step, z_count)
 
     def kv_peer(step):
-        return lax.rem(kv + step, kv_count)
+        return paired(kv, step, kv_count)
+
+    def tp_peer(step):
+        return paired(tp, step, tp_count)
 
     own_rows = pltpu.make_async_copy(tokens_hbm, rows_all.at[tp], load_sem.at[0])
     own_rows.start()
@@ -125,7 +138,7 @@
     barrier = pltpu.get_barrier_semaphore()
     for step in range(1, tp_count):
         pl.semaphore_signal(
-            barrier, inc=1, device_id=(kv, lax.rem(tp + step, tp_count)), device_id_type=MESH
+            barrier, inc=1, device_id=(kv, tp_peer(step)), device_id_type=MESH
         )
     for step in range(1, kv_count):
         pl.semaphore_signal(barrier, inc=1, device_id=(kv_peer(step), tp), device_id_type=MESH)
@@ -133,63 +146,48 @@
 
     own_rows.wait()
     sent = []
-    for step in range(1, tp_count):
+    for step in range(tp_count - 1, 0, -1):
         copy = remote(
             rows_all.at[tp],
             rows_all.at[tp],
             rows_send.at[step],
             rows_recv.at[tp],
             kv,
-            lax.rem(tp + step, tp_count),
+            tp_peer(step),
         )
         copy.start()
         sent.append(copy)
-    for step in range(1, tp_count):
-        source = lax.rem(tp + step, tp_count)
-        remote(
-            rows_all.at[source],
-            rows_all.at[source],
-            rows_send.at[step],
-            rows_recv.at[source],
-            kv,
-            source,
-        ).wait_recv()
-
     loads[0].wait()
     loads[1].wait()
     squares = jnp.zeros((count, width), jnp.float32)
     write_sums = [jnp.zeros((count, width), jnp.float32) for _ in range(heads)]
     decay_sums = [jnp.zeros((count, width), jnp.float32) for _ in range(heads)]
-    scaled = []
-    for block in range(tp_count):
-        columns = slice(block * width, (block + 1) * width)
-        floats = rows_all[block].astype(jnp.float32)
+    sums = [jnp.zeros((count, heads * size), jnp.float32) for _ in range(4)]
+    for step in range(tp_count):
+        source = tp_peer(step)
+        if step > 0:
+            remote(
+                rows_all.at[source],
+                rows_all.at[source],
+                rows_send.at[step],
+                rows_recv.at[source],
+                kv,
+                source,
+            ).wait_recv()
+        here = pl.ds(pl.multiple_of(source * width, width), width)
+        floats = rows_all[source].astype(jnp.float32)
         squares += floats * floats
-        floats = floats * attn_gain[:, columns]
+        floats = floats * attn_gain[:, here]
         for head in range(heads):
-            write_sums[head] += floats * w_rates[0, head : head + 1, columns].astype(jnp.float32)
-            decay_sums[head] += floats * w_rates[1, head : head + 1, columns].astype(jnp.float32)
-        scaled.append(floats.astype(jnp.bfloat16))
+            write_sums[head] += floats * w_rates[0, head : head + 1, here].astype(jnp.float32)
+            decay_sums[head] += floats * w_rates[1, head : head + 1, here].astype(jnp.float32)
+        scaled = floats.astype(jnp.bfloat16)
+        for index, weight in enumerate((w_query, w_key, w_value, w_outgate)):
+            if step == 0:
+                loads[2 + index].wait()
+            sums[index] += jnp.dot(scaled, weight[here, :], preferred_element_type=jnp.float32)
     norm = lax.rsqrt(jnp.sum(squares, axis=-1, keepdims=True) / model + EPS)
-
-    def project(weight):
-        product = jnp.zeros((count, heads * size), jnp.float32)
-        for block in range(tp_count):
-            product += jnp.dot(
-                scaled[block],
-                weight[block * width : (block + 1) * width, :],
-                preferred_element_type=jnp.float32,
-            )
-        return product * norm
-
-    loads[2].wait()
-    query = project(w_query)
-    loads[3].wait()
-    key = project(w_key)
-    loads[4].wait()
-    value = project(w_value)
-    loads[5].wait()
-    gate_in = project(w_outgate)
+    query, key, value, gate_in = [part * norm for part in sums]
 
     loads[6].wait()
     mixed = []
@@ -219,7 +217,7 @@
             recalled = jnp.sum(carried * key_column, axis=0, keepdims=True)
             fresh = strength[here, :] * (value[here, lanes] - recalled)
             updated = carried + key_column * fresh
-            state[row, head] = updated
+            new_state[row, head] = updated
             rows.append(jnp.sum(updated * query_t[:, here], axis=0, keepdims=True))
         readout = jnp.concatenate(rows, axis=0)
         normed_out = readout * lax.rsqrt(
@@ -228,8 +226,6 @@
         gate_h = gate_in[:, lanes]
         silu = gate_h / (1.0 + jnp.exp(-gate_h))
         mixed.append((normed_out * head_gain_ref[:, lanes] * silu).astype(jnp.bfloat16))
-    store = pltpu.make_async_copy(state, new_state_hbm, store_sem)
-    store.start()
 
     loads[7].wait()
 
@@ -244,8 +240,8 @@
             )
         return product
 
-    for step in range(1, tp_count):
-        owner = lax.rem(tp + step, tp_count)
+    for step in range(tp_count - 1, 0, -1):
+        owner = tp_peer(step)
         share_out[step] = out_block(owner).astype(jnp.bfloat16)
         copy = remote(
             share_out.at[step],
@@ -259,7 +255,7 @@
         sent.append(copy)
     residual = rows_all[tp].astype(jnp.float32) + out_block(tp)
     for step in range(1, tp_count):
-        source = lax.rem(tp + step, tp_count)
+        source = tp_peer(step)
         remote(
             share_out.at[step],
             share_in.at[source],
@@ -294,15 +290,15 @@
             partner,
         ).wait_recv()
 
-    for step in range(1, z_count):
+    for step in range(z_count - 1, 0, -1):
         pass_on(tp, kv, res_send_z.at[step], kv, 2 * z_peer(step) + core)
-    for step in range(1, kv_count):
+    for step in range(kv_count - 1, 0, -1):
         pass_on(tp, kv, res_send_kv.at[0, step], kv_peer(step), tp)
     pass_on(tp, kv, res_send_pair.at[0, 0], kv, partner)
     for z_step in range(1, z_count):
         block = 2 * z_peer(z_step) + core
         arrival(block, kv)
-        for step in range(1, kv_count):
+        for step in range(kv_count - 1, 0, -1):
             pass_on(block, kv, res_send_kv.at[z_step, step], kv_peer(step), tp)
         pass_on(block, kv, res_send_pair.at[z_step, 0], kv, partner)
     for z_step in range(z_count):
@@ -310,10 +306,6 @@
         for step in range(1, kv_count):
             arrival(block, kv_peer(step))
             pass_on(block, kv_peer(step), res_send_pair.at[z_step, step], kv, partner)
-    for z_step in range(z_count):
-        block = 2 * z_peer(z_step) + 1 - core
-        for step in range(kv_count):
-            arrival(block, kv_peer(step))
 
     everyone = kv_count * count
     units = w_gate_hbm.shape[0]
@@ -322,15 +314,20 @@
     squares = jnp.zeros((everyone, width), jnp.float32)
     gate_pre = jnp.zeros((everyone, units), jnp.float32)
     up_pre = jnp.zeros((everyone, units), jnp.float32)
-    for block in range(tp_count):
-        columns = slice(block * width, (block + 1) * width)
-        floats = res_all[block].reshape(everyone, width).astype(jnp.float32)
-        squares += floats * floats
-        part = (floats * mlp_gain[:, columns]).astype(jnp.bfloat16)
-        gate_pre += lax.dot_general(
-            part, w_gate[:, columns], NT, preferred_element_type=jnp.float32
-        )
-        up_pre += lax.dot_general(part, w_up[:, columns], NT, preferred_element_type=jnp.float32)
+    for side in range(2):
+        for z_step in range(z_count):
+            block = 2 * z_peer(z_step) + core + side * (1 - 2 * core)
+            if side == 1:
+                for step in range(kv_count):
+                    arrival(block, kv_peer(step))
+            here = pl.ds(pl.multiple_of(block * width, width), width)
+            floats = res_all[block].reshape(everyone, width).astype(jnp.float32)
+            squares += floats * floats
+            part = (floats * mlp_gain[:, here]).astype(jnp.bfloat16)
+            gate_pre += lax.dot_general(
+                part, w_gate[:, here], NT, preferred_element_type=jnp.float32
+            )
+            up_pre += lax.dot_general(part, w_up[:, here], NT, preferred_element_type=jnp.float32)
     norm = lax.rsqrt(jnp.sum(squares, axis=-1, keepdims=True) / model + EPS)
     gate_pre = gate_pre * norm
     hidden = (gate_pre / (1.0 + jnp.exp(-gate_pre)) * (up_pre * norm)).astype(jnp.bfloat16)
@@ -341,7 +338,8 @@
         product = jnp.dot(hidden, w_down[:, columns], preferred_element_type=jnp.float32)
         return product.reshape(kv_count, count, width)
 
-    for step in range(z_count):
+    order = list(range(z_count - 1, -1, -1))
+    for step in order:
         there = z_peer(step)
         pair_out[step] = down_block(2 * there + 1 - core).astype(jnp.bfloat16)
         copy = remote(
@@ -354,10 +352,9 @@
         )
         copy.start()
         sent.append(copy)
-    for step in range(z_count):
+    for step in order:
         there = z_peer(step)
         total[there] = down_block(2 * there + core)
-    order = [step for step in range(1, z_count)] + [0]
     for step in order:
         there = z_peer(step)
         remote(
@@ -368,7 +365,7 @@
             kv,
             partner,
         ).wait_recv()
-        for kv_step in range(1, kv_count):
+        for kv_step in range(kv_count - 1, 0, -1):
             group = kv_peer(kv_step)
             both = total[there, group] + pair_in[there, group].astype(jnp.float32)
             group_out[there, group] = both.astype(jnp.bfloat16)
@@ -427,7 +424,6 @@
 
     for copy in sent:
         copy.wait_send()
-    store.wait()
 
 
 def body(
@@ -491,7 +487,6 @@
         pltpu.VMEM((z_count, count, width), bf16),
         pltpu.VMEM((z_count, count, width), bf16),
         dma((len(local) + 1,)),
-        dma,
         dma((tp_count,)),
         dma((tp_count,)),
         dma((tp_count,)),
@@ -510,11 +505,11 @@
     return pl.pallas_call(
         functools.partial(layer_kernel, kv_count, tp_count),
         out_shape=(
-            jax.ShapeDtypeStruct(tokens.shape, bf16),
-            jax.ShapeDtypeStruct(state.shape, jnp.float32),
+            pltpu.VMEM(tokens.shape, bf16),
+            pltpu.VMEM(state.shape, jnp.float32),
         ),
         in_specs=[vmem if index in in_vmem else anywhere for index in range(len(operands))],
-        out_specs=(vmem, anywhere),
+        out_specs=(vmem, vmem),
         scratch_shapes=local + exchange,
         compiler_params=pltpu.CompilerParams(
             collective_id=0, has_side_effects=True, vmem_limit_bytes=60 * 1024 * 1024

time: 47.4 us -> 40.9 us (0.86)
  Pallas kernels: 42 us -> 38.1 us
  local copies, waits for them, and re-layouts: 4.46 us -> 1.93 us
    pallas_call x1, Pallas kernels: 42 us -> 38.1 us  [body(): pl.pallas_call(functools.partial(layer_kernel, kv_count, tp_count), out_s...]
    unnamed x2, local copies, waits for them, and re-layouts: 4.46 us -> 1.93 us
where the time goes in v2:
time: 40.9 us; the launch traced here: 40.7 us
  Pallas kernels  38.1 us (93%)
  local copies, waits for them, and re-layouts  1.93 us (5%)
  between operations  0.64 us (2%)
    pallas_call x1, Pallas kernels, body(): pl.pallas_call(functools.partial(layer_kernel, kv_count, tp_count), out_s...  38.1 us
    unnamed x2, local copies, waits for them, and re-layouts  1.93 us

profile of v2, /device:TPU:0, one launch (start us, length us, event | category | flops | bytes accessed | tf_op | source)
XLA Modules:
  0.0 40.7 jit_solution(16833544389981962040)
XLA Ops:
  0.6 38.1 %layer.1 = (bf16[16,512]{1,0:T(8,128)(2,1)S(1)}, f32[16,2,128,128]{3,2,1,0:T(8,128)S(1)}) custom-call(bf16[16,512]{1,0:T(8,128)(2,1)} %tokens_hbm.1, f32[1,4096]{1,0:T(1,128)} %bitcast.12, bf16[4096,256]{1,0:T(8,128)(2,1)} %w_query_hbm.1, bf16[4096,256]{1,0:T(8,128)(2,1)} %w_key_hbm.1, bf16[4096,256]{1,0:T(8,128)(2,1)} %w_value_hbm.1, ...), custom_call_target="tpu_custom_call" | custom-call | tf_op jit(solution)/shard_map/layer/pallas_call | solution.py:505
  38.7 0.6 %copy.19 = bf16[16,512]{1,0:T(8,128)(2,1)} copy(bf16[16,512]{1,0:T(8,128)(2,1)S(1)} %get-tuple-element.2) | data formatting | bytes 32768
  39.4 1.3 %copy.20 = f32[16,2,128,128]{3,2,1,0:T(8,128)} copy(f32[16,2,128,128]{3,2,1,0:T(8,128)S(1)} %get-tuple-element.3) | data formatting | bytes 4194304
